TPU v7x, 32 devices: a whole 2x2x4 slice. The times are simulated.
32 devices in a mesh: grp: 2 (over y), sp: 4 (over z), tp: 4 (over x, core).
Axes of the slice: x: 2, y: 2, z: 4, core: 2. Of those that a mesh axis runs over, the one named last changes fastest.
Arguments:
- hidden_in: bfloat16 [3072, 4096], P(('grp', 'sp'), 'tp'), parts along dimension 0, may hold values from -30 to 30
- in_gain: float32 [2, 4096], P(None, 'tp'), may hold values from 0.1 to 1.9
- w_value: bfloat16 [2, 4096, 2048], P(None, 'sp', 'tp'), may hold values from -0.09375 to 0.09375
- w_gate: bfloat16 [2, 4096, 2048], P(None, 'sp', 'tp'), may hold values from -0.09375 to 0.09375
- conv_taps: float32 [2, 31, 2048], P(None, None, 'tp'), may hold values from -9 to 9
- norm_gain: float32 [2, 2048], P(None, 'tp'), may hold values from 0.1 to 1.9
- norm_shift: float32 [2, 2048], P(None, 'tp'), may hold values from -3 to 3
- w_out: bfloat16 [2, 2048, 4096], P(None, 'tp', 'sp'), may hold values from -0.125 to 0.125
Outputs:
- hidden_out: bfloat16 [3072, 4096], P(('grp', 'sp'), 'tp'), parts along dimension 0
There are 2 independent parts, one for each index of `grp`. A program takes and returns all parts, laid end to end along the dimension named above; an argument that names none is the same for every part. Nothing has to cross between parts.
All inputs are finite; a program needn't handle non-finite values.
Results may differ from a plain program's by a relative error of at most 0.013.
Values may be sent and summed in bfloat16 or wider, within the bound.
A program may use at most 64 MiB of HBM per device.

v0:
```python
import jax
import jax.numpy as jnp
from jax import lax
from jax.sharding import PartitionSpec as P

D = 4096
C = 2048
epsilon = 1e-06


def passed_along(value, axis, steps):
    count = lax.axis_size(axis)
    initial, last = (max(0, -steps), min(count, count - steps))
    return lax.ppermute(value, axis, [(source, source + steps) for source in range(initial, last)])


def depthwise(extended, kernel_taps):
    conved = lax.conv_general_dilated(
        extended.astype(jnp.float32)[None],
        kernel_taps[:, None, :],
        (1,),
        [(0, 0)],
        dimension_numbers=("NWC", "WIO", "NWC"),
        feature_group_count=extended.shape[1],
        precision=lax.Precision.HIGHEST,
    )
    return conved[0]


def shards(hidden_in, in_gain, w_value, w_gate, conv_taps, norm_gain, norm_shift, w_out):
    layer_count = w_value.shape[0]
    reach_rows = conv_taps.shape[1] - 1
    value_all, gate_all = (
        lax.all_gather(w_value, "sp", axis=1, tiled=True),
        lax.all_gather(w_gate, "sp", axis=1, tiled=True),
    )
    out_all = lax.all_gather(w_out, "sp", axis=2, tiled=True)
    current = hidden_in
    for layer_idx in range(layer_count):
        widened = current.astype(jnp.float32)
        squares = lax.psum(jnp.sum(widened * widened, axis=1), "tp")
        normalized = (
            widened * lax.rsqrt(squares / D + epsilon)[:, None] * in_gain[layer_idx]
        ).astype(jnp.bfloat16)
        gathered = lax.all_gather(normalized, "tp", axis=1, tiled=True)
        value_part = jnp.dot(gathered, value_all[layer_idx], preferred_element_type=jnp.float32)
        gate_part = jnp.dot(gathered, gate_all[layer_idx], preferred_element_type=jnp.float32)
        gated = (value_part * jax.nn.sigmoid(gate_part)).astype(jnp.bfloat16)
        before = passed_along(gated[gated.shape[0] - reach_rows :], "sp", 1)
        extended = jnp.concatenate([before, gated], axis=0)
        residual = current
        conved = depthwise(extended, conv_taps[layer_idx])
        total_sum, total_squares = lax.psum(
            (jnp.sum(conved, axis=1), jnp.sum(conved * conved, axis=1)), "tp"
        )
        row_mean = total_sum / C
        spread = total_squares / C - row_mean * row_mean
        normed = (conved - row_mean[:, None]) * lax.rsqrt(spread + epsilon)[:, None] * norm_gain[
            layer_idx
        ] + norm_shift[layer_idx]
        mixed_out = jax.nn.silu(normed).astype(jnp.bfloat16)
        partial_value = jnp.dot(mixed_out, out_all[layer_idx], preferred_element_type=jnp.float32)
        summed = lax.psum_scatter(
            partial_value.astype(jnp.bfloat16), "tp", scatter_dimension=1, tiled=True
        ).astype(jnp.float32)
        current = (residual.astype(jnp.float32) + summed).astype(jnp.bfloat16)
    return current


def solution(mesh):
    placed = (
        P(("grp", "sp"), "tp"),
        P(None, "tp"),
        P(None, "sp", "tp"),
        P(None, "sp", "tp"),
        P(None, None, "tp"),
        P(None, "tp"),
        P(None, "tp"),
        P(None, "tp", "sp"),
    )
    return jax.shard_map(
        shards, mesh=mesh, in_specs=placed, out_specs=P(("grp", "sp"), "tp"), check_vma=False
    )
```

profile of v0, /device:TPU:0, one launch (start us, length us, event | category | flops | bytes accessed | tf_op | source)
XLA Modules:
  0.0 657.1 jit_solution(9422213232833642842)
XLA Ops:
  6.5 1.4 fusion.4
  7.9 8.4 %psum.42 = f32[384]{0:T(512)S(1)} all-reduce(f32[384]{0:T(512)S(1)} %fusion.4), channel_id=1, replica_groups=mesh['grp'=2,'sp'=4,'tp'=4] {'tp'}, use_global_device_ids=true, to_apply=%region_1.0 | all-reduce | flops 384 | bytes 3072 | tf_op jit(solution)/shard_map/psum | solution.py:41
  16.3 0.8 fusion.62
  17.1 2.3 fusion.6
  19.4 0.7 all-gather.10.cloned.1.call-update
  20.2 0.7 all-gather.8.cloned.1.call-update
  20.9 0.5 all-gather.12.cloned.1.call-update
  21.5 26.8 %all-gather.6.cloned.1.call-done = bf16[384,4096]{1,0:T(8,128)(2,1)} async-done(((bf16[384,1024]{1,0:T(8,128)(2,1)}), bf16[384,4096]{1,0:T(8,128)(2,1)}) %all-gather.6.cloned.1.call-update) | async-done | bytes 3145744 | tf_op jit(solution)/shard_map/all_gather | solution.py:45
  48.3 151.2 %all-gather.10.cloned.1.call-done = bf16[2,4096,512]{2,1,0:T(8,128)(2,1)} async-done(((bf16[2,1024,512]{2,1,0:T(8,128)(2,1)}), bf16[2,4096,512]{2,1,0:T(8,128)(2,1)}) %all-gather.10.cloned.1.call-update) | async-done | bytes 8388624 | tf_op jit(solution)/shard_map/all_gather | solution.py:35
  199.5 5.9 fusion.23
  205.5 143.5 %all-gather.8.cloned.1.call-done = bf16[2,4096,512]{2,1,0:T(8,128)(2,1)} async-done(((bf16[2,1024,512]{2,1,0:T(8,128)(2,1)}), bf16[2,4096,512]{2,1,0:T(8,128)(2,1)}) %all-gather.8.cloned.1.call-update) | async-done | bytes 8388624 | tf_op jit(solution)/shard_map/all_gather | solution.py:34
  349.0 4.2 fusion.25
  353.2 1.4 collective-permute-start
  354.6 1.6 collective-permute-done
  356.2 0.1 maximum_bitcast_fusion
  356.4 0.1 copy.14
  356.6 1.9 fusion.65
  358.5 0.5 copy.16
  359.0 0.1 reshape.62
  359.1 0.5 copy.15
  359.6 0.1 reshape.60
  359.7 0.2 slice_reduce_fusion.1
  359.9 6.6 all-reduce.1
  366.5 131.7 %all-gather.12.cloned.1.call-done = bf16[2,512,4096]{2,1,0:T(8,128)(2,1)} async-done(((bf16[2,512,1024]{2,1,0:T(8,128)(2,1)}), bf16[2,512,4096]{2,1,0:T(8,128)(2,1)}) %all-gather.12.cloned.1.call-update) | async-done | bytes 8388624 | tf_op jit(solution)/shard_map/all_gather | solution.py:37
  498.2 5.9 convolution_convert_fusion.1
  504.2 36.0 %reduce-scatter.3.cloned.1.call-done = bf16[384,1024]{1,0:T(8,128)(2,1)} async-done(((bf16[384,4096]{1,0:T(8,128)(2,1)}), bf16[384,1024]{1,0:T(8,128)(2,1)}) %reduce-scatter.3.cloned.1.call-update) | async-done | bytes 786448 | tf_op jit(solution)/shard_map/reduce_scatter | solution.py:63
  540.2 1.5 fusion.8
  541.6 5.8 psum.45
  547.4 2.3 fusion.10
  549.8 0.2 reduce-scatter.5.cloned.1.call-start
  550.0 29.1 %all-gather.14.cloned.1.call-done = bf16[384,4096]{1,0:T(8,128)(2,1)} async-done(((bf16[384,1024]{1,0:T(8,128)(2,1)}), bf16[384,4096]{1,0:T(8,128)(2,1)}) %all-gather.14.cloned.1.call-update) | async-done | bytes 3145744 | tf_op jit(solution)/shard_map/all_gather | solution.py:45
  579.0 5.2 fusion.21
  584.2 4.0 fusion.24
  588.3 3.4 collective-permute-start.1
  591.7 1.6 collective-permute-done.1
  593.3 0.1 maximum_bitcast_fusion.1
  593.5 0.1 copy.18
  593.7 2.0 fusion.66
  595.7 0.5 copy.20
  596.2 0.1 reshape.71
  596.3 0.1 slice_reduce_fusion
  596.5 0.5 copy.19
  597.0 0.1 reshape.69
  597.1 0.1 slice_reduce_fusion.2
  597.2 5.9 all-reduce
  603.2 5.9 convolution_convert_fusion
  609.1 38.7 %reduce-scatter.5.cloned.1.call-done = bf16[384,1024]{1,0:T(8,128)(2,1)} async-done(((bf16[384,4096]{1,0:T(8,128)(2,1)}), bf16[384,1024]{1,0:T(8,128)(2,1)}) %reduce-scatter.5.cloned.1.call-update) | async-done | bytes 786448 | tf_op jit(solution)/shard_map/reduce_scatter | solution.py:63
  647.8 2.4 fusion.11
  (40 shorter events, 0.7 us)
Async XLA Ops:
  6.5 41.8 %all-gather.6.cloned.1.call-start = ((), (), s32[]{:S(2)}) async-start(), calls=%async_computation.2 | async-start | bytes 3932160 | tf_op jit(solution)/shard_map/all_gather | solution.py:45
  19.4 2.1 copy-start.2
  19.4 180.2 %all-gather.10.cloned.1.call-start = ((), (), s32[]{:S(2)}) async-start(), calls=%async_computation.4 | async-start | bytes 10485760 | tf_op jit(solution)/shard_map/all_gather | solution.py:35
  20.1 328.8 %all-gather.8.cloned.1.call-start = ((), (), s32[]{:S(2)}) async-start(), calls=%async_computation.3 | async-start | bytes 10485760 | tf_op jit(solution)/shard_map/all_gather | solution.py:34
  20.9 477.4 %all-gather.12.cloned.1.call-start = ((), (), s32[]{:S(2)}) async-start(), calls=%async_computation.5 | async-start | bytes 10485760 | tf_op jit(solution)/shard_map/all_gather | solution.py:37
  21.4 518.8 %reduce-scatter.3.cloned.1.call-start = ((), (), s32[]{:S(2)}) async-start(), calls=%async_computation.6 | async-start | bytes 3932160 | tf_op jit(solution)/shard_map/reduce_scatter | solution.py:63
  48.3 300.6 %copy-start.4 = (bf16[384,4096]{1,0:T(8,128)(2,1)S(1)}, bf16[384,4096]{1,0:T(8,128)(2,1)}, u32[]{:S(2)}) copy-start(bf16[384,4096]{1,0:T(8,128)(2,1)} %all-gather.6.cloned.1.call-done) | copy-start | bytes 9437188
  205.5 149.1 %copy-start.3 = (f32[2,512]{1,0:T(2,128)S(1)}, f32[2,512]{1,0:T(2,128)}, u32[]{:S(2)}) copy-start(f32[2,512]{1,0:T(2,128)} %param.14) | copy-start | bytes 12292
  353.1 3.5 copy-start.6
  353.2 3.5 copy-start.7
  353.2 3.0 collective-permute-start
  504.1 36.1 %copy-start = (bf16[384,1024]{1,0:T(8,128)(2,1)S(1)}, bf16[384,1024]{1,0:T(8,128)(2,1)}, u32[]{:S(2)}) copy-start(bf16[384,1024]{1,0:T(8,128)(2,1)} %param.8) | copy-start | bytes 2359300
  504.1 74.9 %all-gather.14.cloned.1.call-start = ((), (), s32[]{:S(2)}) async-start(), calls=%async_computation.7 | async-start | bytes 3932160 | tf_op jit(solution)/shard_map/all_gather | solution.py:45
  549.8 98.0 %reduce-scatter.5.cloned.1.call-start = ((), (), s32[]{:S(2)}) async-start(), calls=%async_computation.8 | async-start | bytes 3932160 | tf_op jit(solution)/shard_map/reduce_scatter | solution.py:63
  579.0 5.2 copy-start.5
  588.3 5.0 collective-permute-start.1
  609.1 38.7 %copy-start.1 = (bf16[384,1024]{1,0:T(8,128)(2,1)S(1)}, bf16[384,1024]{1,0:T(8,128)(2,1)}, u32[]{:S(2)}) copy-start(bf16[384,1024]{1,0:T(8,128)(2,1)} %reduce-scatter.3.cloned.1.call-done) | copy-start | bytes 2359300
Sparse Core Ops, SparseCore 0:
  19.5 28.8 all-gather.5
  49.9 149.6 all-gather.9
  201.1 147.7 all-gather.7
  350.4 147.7 all-gather.11
  504.2 35.8 reduce-scatter.2
  549.9 29.1 all-gather.13
  609.2 38.5 reduce-scatter.4
where the time goes:
time: 658 us; the launch traced here: 657 us
  waiting for transfers between devices  562 us (85%)
  matrix products  35 us (5%)
  blocking collectives  26.6 us (4%)
  between operations  13.8 us (2%)
  other arithmetic  10.6 us (2%)
    all_gather x1, waiting for transfers between devices, shards(): lax.all_gather(w_gate, 'sp', axis=1, tiled=True)  151 us
    all_gather x1, waiting for transfers between devices, shards(): lax.all_gather(w_value, 'sp', axis=1, tiled=True)  143 us
    all_gather x1, waiting for transfers between devices, shards(): out_all = lax.all_gather(w_out, 'sp', axis=2, tiled=True)  132 us
    reduce_scatter x2, waiting for transfers between devices, shards(): lax.psum_scatter(partial_value.astype(jnp.bfloat16), 'tp', scatter_dimens...  74.7 us
    all_gather x2, waiting for transfers between devices, shards(): gathered = lax.all_gather(normalized, 'tp', axis=1, tiled=True)  55.9 us
    psum x2, blocking collectives, shards(): squares = lax.psum(jnp.sum(widened * widened, axis=1), 'tp')  14.1 us
  transfers between devices with their start and end apart: 9, of which 9 were waited for; matrix products, arithmetic and copies ran while one was open for 2% of the time, Pallas kernels for 0%

commit v1 on v0

--- a/solution.py
+++ b/solution.py
@@ -34,7 +34,13 @@
         lax.all_gather(w_value, "sp", axis=1, tiled=True),
         lax.all_gather(w_gate, "sp", axis=1, tiled=True),
     )
-    out_all = lax.all_gather(w_out, "sp", axis=2, tiled=True)
+    size = lax.axis_size("sp")
+    block, blocks = (w_out, [w_out])
+    for _ in range(size - 1):
+        block = lax.ppermute(block, "sp", [(i, (i + 1) % size) for i in range(size)])
+        blocks.insert(0, block)
+    flat = jnp.concatenate(blocks, axis=2)
+    out_all = jnp.roll(flat, (lax.axis_index("sp") + 1) * w_out.shape[2], axis=2)
     current = hidden_in
     for layer_idx in range(layer_count):
         widened = current.astype(jnp.float32)

time: 658 us -> 611 us (0.929)
  waiting for transfers between devices: 562 us -> 433 us
  starting transfers between devices: 5.24 us -> 67.2 us
  local copies, waits for them, and re-layouts: 3.79 us -> 23.5 us
    ppermute x0 -> x3, waiting for transfers between devices: none -> 216 us  [shards(): lax.ppermute(block, 'sp', [(i, (i + 1) % size) for i in range(size)])]
    all_gather x1, waiting for transfers between devices: 151 us -> 0.01 us  [shards(): lax.all_gather(w_gate, 'sp', axis=1, tiled=True)]
    all_gather x1 -> x0, waiting for transfers between devices: 132 us -> none  [shards(): out_all = lax.all_gather(w_out, 'sp', axis=2, tiled=True)]
    ppermute x0 -> x3, starting transfers between devices: none -> 61.8 us  [shards(): lax.ppermute(block, 'sp', [(i, (i + 1) % size) for i in range(size)])]
    all_gather x1, waiting for transfers between devices: 143 us -> 108 us  [shards(): lax.all_gather(w_value, 'sp', axis=1, tiled=True)]
    all_gather x2, waiting for transfers between devices: 55.9 us -> 29.1 us  [shards(): gathered = lax.all_gather(normalized, 'tp', axis=1, tiled=True)]
    unnamed x16 -> x27, local copies, waits for them, and re-layouts: 0.04 us -> 18.3 us
  transfers between devices with their start and end apart: 9 -> 11, of which waited for: 9 -> 9; matrix products, arithmetic and copies ran while one was open for 2% -> 4% of each run, Pallas kernels for 0% -> 0%
where the time goes in v1:
time: 611 us; the launch traced here: 610 us
  waiting for transfers between devices  433 us (71%)
  starting transfers between devices  67.2 us (11%)
  matrix products  34.8 us (6%)
  blocking collectives  26.6 us (4%)
  local copies, waits for them, and re-layouts  23.5 us (4%)
  between operations  13.8 us (2%)
  other arithmetic  10.8 us (2%)
    ppermute x3, waiting for transfers between devices, shards(): lax.ppermute(block, 'sp', [(i, (i + 1) % size) for i in range(size)])  216 us
    all_gather x1, waiting for transfers between devices, shards(): lax.all_gather(w_value, 'sp', axis=1, tiled=True)  108 us
    reduce_scatter x2, waiting for transfers between devices, shards(): lax.psum_scatter(partial_value.astype(jnp.bfloat16), 'tp', scatter_dimens...  77.6 us
    ppermute x3, starting transfers between devices, shards(): lax.ppermute(block, 'sp', [(i, (i + 1) % size) for i in range(size)])  61.8 us
    all_gather x2, waiting for transfers between devices, shards(): gathered = lax.all_gather(normalized, 'tp', axis=1, tiled=True)  29.1 us
    unnamed x27, local copies, waits for them, and re-layouts  18.3 us
    psum x2, blocking collectives, shards(): squares = lax.psum(jnp.sum(widened * widened, axis=1), 'tp')  14.1 us
    psum x2, blocking collectives, shards(): lax.psum((jnp.sum(conved, axis=1), jnp.sum(conved * conved, axis=1)), 'tp')  12.5 us
  transfers between devices with their start and end apart: 11, of which 9 were waited for; matrix products, arithmetic and copies ran while one was open for 4% of the time, Pallas kernels for 0%

profile of v1, /device:TPU:0, one launch (start us, length us, event | category | flops | bytes accessed | tf_op | source)
XLA Modules:
  0.0 609.8 jit_solution(9408921119890468791)
XLA Ops:
  6.5 0.8 fusion.64
  7.3 1.4 fusion.4
  8.7 8.4 %psum.42 = f32[384]{0:T(512)S(1)} all-reduce(f32[384]{0:T(512)S(1)} %fusion.4), channel_id=1, replica_groups=mesh['grp'=2,'sp'=4,'tp'=4] {'tp'}, use_global_device_ids=true, to_apply=%region_1.2 | all-reduce | flops 384 | bytes 3072 | tf_op jit(solution)/shard_map/psum | solution.py:47
  17.1 2.4 fusion.6
  19.6 0.7 all-gather.9.cloned.1.call-update
  20.3 0.7 all-gather.7.cloned.1.call-update
  21.1 1.6 collective-permute-start.1
  22.7 53.8 %collective-permute-done.1 = bf16[2,512,1024]{2,1,0:T(8,128)(2,1)S(1)} collective-permute-done((bf16[2,512,1024]{2,1,0:T(8,128)(2,1)S(1)}, bf16[2,512,1024]{2,1,0:T(8,128)(2,1)S(1)}, u32[]{:S(2)}, u32[]{:S(2)}) %collective-permute-start.1) | collective-permute-done | bytes 2097184 | tf_op jit(solution)/shard_map/ppermute | solution.py:40
  76.5 1.3 copy-done.2
  77.9 9.7 %collective-permute-start.2 = (bf16[2,512,1024]{2,1,0:T(8,128)(2,1)S(1)}, bf16[2,512,1024]{2,1,0:T(8,128)(2,1)}, u32[]{:S(2)}, u32[]{:S(2)}) collective-permute-start(bf16[2,512,1024]{2,1,0:T(8,128)(2,1)S(1)} %collective-permute-done.1), channel_id=1, source_target_pairs={{0,4},{4,8},{8,12},{12,0},{1,5},{5,9},{9,13},{13,1},{2,6},{6,10},{... | collective-permute-start | bytes 6291464 | tf_op jit(solution)/shard_map/ppermute | solution.py:40
  87.6 89.0 %collective-permute-done.2 = bf16[2,512,1024]{2,1,0:T(8,128)(2,1)} collective-permute-done((bf16[2,512,1024]{2,1,0:T(8,128)(2,1)S(1)}, bf16[2,512,1024]{2,1,0:T(8,128)(2,1)}, u32[]{:S(2)}, u32[]{:S(2)}) %collective-permute-start.2) | collective-permute-done | bytes 2097184 | tf_op jit(solution)/shard_map/ppermute | solution.py:40
  176.6 50.4 %collective-permute-start.3 = (bf16[2,512,1024]{2,1,0:T(8,128)(2,1)}, bf16[2,512,1024]{2,1,0:T(8,128)(2,1)}, u32[]{:S(2)}, u32[]{:S(2)}) collective-permute-start(bf16[2,512,1024]{2,1,0:T(8,128)(2,1)} %collective-permute-done.2), channel_id=1, source_target_pairs={{0,4},{4,8},{8,12},{12,0},{1,5},{5,9},{9,13},{13,1},{2,6},{6,10},{... | collective-permute-start | bytes 6291464 | tf_op jit(solution)/shard_map/ppermute | solution.py:40
  227.1 72.8 %collective-permute-done.3 = bf16[2,512,1024]{2,1,0:T(8,128)(2,1)} collective-permute-done((bf16[2,512,1024]{2,1,0:T(8,128)(2,1)}, bf16[2,512,1024]{2,1,0:T(8,128)(2,1)}, u32[]{:S(2)}, u32[]{:S(2)}) %collective-permute-start.3) | collective-permute-done | bytes 2097184 | tf_op jit(solution)/shard_map/ppermute | solution.py:40
  299.9 3.1 constant_dynamic-update-slice_fusion.7
  303.0 3.1 constant_dynamic-update-slice_fusion.6
  306.1 1.5 constant_dynamic-update-slice_fusion.5
  307.6 1.5 constant_dynamic-update-slice_fusion.4
  309.1 3.1 constant_dynamic-update-slice_fusion.3
  312.2 3.1 constant_dynamic-update-slice_fusion.2
  315.3 1.5 constant_dynamic-update-slice_fusion.1
  316.8 5.1 fusion.23
  321.9 107.8 %all-gather.7.cloned.1.call-done = bf16[2,4096,512]{2,1,0:T(8,128)(2,1)} async-done(((bf16[2,1024,512]{2,1,0:T(8,128)(2,1)}), bf16[2,4096,512]{2,1,0:T(8,128)(2,1)}) %all-gather.7.cloned.1.call-update) | async-done | bytes 8388624 | tf_op jit(solution)/shard_map/all_gather | solution.py:34
  429.7 4.9 fusion.25
  434.7 1.7 collective-permute-start
  436.4 1.5 constant_dynamic-update-slice_fusion
  438.4 1.9 fusion.67
  440.3 0.5 copy.15
  440.9 0.5 copy.16
  441.5 0.2 slice_reduce_fusion.1
  441.7 6.5 %all-reduce.1 = (f32[384]{0:T(512)S(1)}, f32[384]{0:T(512)S(1)}) all-reduce(f32[384]{0:T(512)S(1)} %get-tuple-element.23, f32[384]{0:T(512)S(1)} %get-tuple-element.24), channel_id=1, replica_groups=mesh['grp'=2,'sp'=4,'tp'=4] {'tp'}, use_global_device_ids=true, to_apply=%region_5.6 | all-reduce | flops 768 | bytes 6144 | tf_op jit(solution)/shard_map/psum | solution.py:59
  448.2 5.8 convolution_convert_fusion.1
  454.1 38.9 %reduce-scatter.3.cloned.1.call-done = bf16[384,1024]{1,0:T(8,128)(2,1)} async-done(((bf16[384,4096]{1,0:T(8,128)(2,1)}), bf16[384,1024]{1,0:T(8,128)(2,1)}) %reduce-scatter.3.cloned.1.call-update) | async-done | bytes 786448 | tf_op jit(solution)/shard_map/reduce_scatter | solution.py:69
  493.0 1.5 fusion.8
  494.5 5.8 psum.45
  500.2 2.3 fusion.10
  502.6 0.2 reduce-scatter.5.cloned.1.call-start
  502.8 29.1 %all-gather.11.cloned.1.call-done = bf16[384,4096]{1,0:T(8,128)(2,1)} async-done(((bf16[384,1024]{1,0:T(8,128)(2,1)}), bf16[384,4096]{1,0:T(8,128)(2,1)}) %all-gather.11.cloned.1.call-update) | async-done | bytes 3145744 | tf_op jit(solution)/shard_map/all_gather | solution.py:51
  531.9 5.2 fusion.21
  537.1 4.0 fusion.24
  541.1 3.4 collective-permute-start.4
  544.5 1.6 collective-permute-done.4
  546.5 2.1 fusion.68
  548.5 0.5 copy.19
  549.1 0.5 copy.20
  550.0 5.9 all-reduce
  556.0 5.8 convolution_convert_fusion
  561.8 38.7 %reduce-scatter.5.cloned.1.call-done = bf16[384,1024]{1,0:T(8,128)(2,1)} async-done(((bf16[384,4096]{1,0:T(8,128)(2,1)}), bf16[384,1024]{1,0:T(8,128)(2,1)}) %reduce-scatter.5.cloned.1.call-update) | async-done | bytes 786448 | tf_op jit(solution)/shard_map/reduce_scatter | solution.py:69
  600.6 2.4 fusion.11
  (55 shorter events, 1.8 us)
Async XLA Ops:
  6.5 310.2 %all-gather.5.cloned.1.call-start = ((), (), s32[]{:S(2)}) async-start(), calls=%async_computation.2 | async-start | bytes 3932160 | tf_op jit(solution)/shard_map/all_gather | solution.py:51
  17.1 4.0 copy-start.1
  17.1 210.0 %copy-start.5 = (f32[2,512]{1,0:T(2,128)S(1)}, f32[2,512]{1,0:T(2,128)}, u32[]{:S(2)}) copy-start(f32[2,512]{1,0:T(2,128)} %param.14) | copy-start | bytes 12292
  17.1 210.0 %copy-start.6 = (f32[2,512]{1,0:T(2,128)S(1)}, f32[2,512]{1,0:T(2,128)}, u32[]{:S(2)}) copy-start(f32[2,512]{1,0:T(2,128)} %param.13) | copy-start | bytes 12292
  19.5 297.3 %all-gather.9.cloned.1.call-start = ((), (), s32[]{:S(2)}) async-start(), calls=%async_computation.4 | async-start | bytes 10485760 | tf_op jit(solution)/shard_map/all_gather | solution.py:35
  20.3 409.4 %all-gather.7.cloned.1.call-start = ((), (), s32[]{:S(2)}) async-start(), calls=%async_computation.3 | async-start | bytes 10485760 | tf_op jit(solution)/shard_map/all_gather | solution.py:34
  21.0 472.0 %reduce-scatter.3.cloned.1.call-start = ((), (), s32[]{:S(2)}) async-start(), calls=%async_computation.5 | async-start | bytes 3932160 | tf_op jit(solution)/shard_map/reduce_scatter | solution.py:69
  21.1 55.5 %collective-permute-start.1 = (bf16[2,512,1024]{2,1,0:T(8,128)(2,1)S(1)}, bf16[2,512,1024]{2,1,0:T(8,128)(2,1)S(1)}, u32[]{:S(2)}, u32[]{:S(2)}) collective-permute-start(bf16[2,512,1024]{2,1,0:T(8,128)(2,1)S(1)} %copy-done.1), channel_id=1, source_target_pairs={{0,4},{4,8},{8,12},{12,0},{1,5},{5,9},{9,13},{13,1},{2,6},{6,10},{... | collective-permute-start | bytes 6291464 | tf_op jit(solution)/shard_map/ppermute | solution.py:40
  76.5 1.3 copy-start.2
  77.9 98.7 %collective-permute-start.2 = (bf16[2,512,1024]{2,1,0:T(8,128)(2,1)S(1)}, bf16[2,512,1024]{2,1,0:T(8,128)(2,1)}, u32[]{:S(2)}, u32[]{:S(2)}) collective-permute-start(bf16[2,512,1024]{2,1,0:T(8,128)(2,1)S(1)} %collective-permute-done.1), channel_id=1, source_target_pairs={{0,4},{4,8},{8,12},{12,0},{1,5},{5,9},{9,13},{13,1},{2,6},{6,10},{... | collective-permute-start | bytes 6291464 | tf_op jit(solution)/shard_map/ppermute | solution.py:40
  176.6 123.3 %collective-permute-start.3 = (bf16[2,512,1024]{2,1,0:T(8,128)(2,1)}, bf16[2,512,1024]{2,1,0:T(8,128)(2,1)}, u32[]{:S(2)}, u32[]{:S(2)}) collective-permute-start(bf16[2,512,1024]{2,1,0:T(8,128)(2,1)} %collective-permute-done.2), channel_id=1, source_target_pairs={{0,4},{4,8},{8,12},{12,0},{1,5},{5,9},{9,13},{13,1},{2,6},{6,10},{... | collective-permute-start | bytes 6291464 | tf_op jit(solution)/shard_map/ppermute | solution.py:40
  227.1 79.1 %copy-start.3 = (bf16[2,512,1024]{2,1,0:T(8,128)(2,1)S(1)}, bf16[2,512,1024]{2,1,0:T(8,128)(2,1)}, u32[]{:S(2)}) copy-start(bf16[2,512,1024]{2,1,0:T(8,128)(2,1)} %copy-done.2) | copy-start | bytes 6291460
  434.7 3.7 copy-start.8
  434.7 3.7 copy-start.9
  434.7 3.3 collective-permute-start
  454.0 38.9 %copy-start = (bf16[384,1024]{1,0:T(8,128)(2,1)S(1)}, bf16[384,1024]{1,0:T(8,128)(2,1)}, u32[]{:S(2)}) copy-start(bf16[384,1024]{1,0:T(8,128)(2,1)} %param.8) | copy-start | bytes 2359300
  454.1 77.8 %all-gather.11.cloned.1.call-start = ((), (), s32[]{:S(2)}) async-start(), calls=%async_computation.6 | async-start | bytes 3932160 | tf_op jit(solution)/shard_map/all_gather | solution.py:51
  502.6 98.0 %reduce-scatter.5.cloned.1.call-start = ((), (), s32[]{:S(2)}) async-start(), calls=%async_computation.7 | async-start | bytes 3932160 | tf_op jit(solution)/shard_map/reduce_scatter | solution.py:69
  531.9 5.2 copy-start.7
  541.1 5.0 collective-permute-start.4
  561.8 38.7 %copy-start.4 = (bf16[384,1024]{1,0:T(8,128)(2,1)S(1)}, bf16[384,1024]{1,0:T(8,128)(2,1)}, u32[]{:S(2)}) copy-start(bf16[384,1024]{1,0:T(8,128)(2,1)} %reduce-scatter.3.cloned.1.call-done) | copy-start | bytes 2359300
Sparse Core Ops, SparseCore 0:
  19.6 28.8 all-gather.4
  50.1 226.9 all-gather.8
  278.7 151.0 all-gather.6
  454.2 38.7 reduce-scatter.2
  502.7 29.1 all-gather.10
  562.0 38.5 reduce-scatter.4
